TPU v7x, 32 devices: a whole 2x2x4 slice. The times are simulated.
32 devices in a mesh: ep: 8 (over z, core), tp: 4 (over y, x).
Axes of the slice: x: 2, y: 2, z: 4, core: 2. Of those that a mesh axis runs over, the one named last changes fastest.
Arguments:
- tokens: bfloat16 [1024, 2048], P('ep', 'tp'), may hold values from -3000 to 3000
- norm_gain: float32 [2048], replicated, may hold values from 0.1 to 1.9
- gate_weight: bfloat16 [8, 2048, 512], P('ep'), may hold values from -0.125 to 0.125
- up_weight: bfloat16 [8, 2048, 512], P('ep'), may hold values from -0.125 to 0.125
- down_weight: bfloat16 [8, 512, 2048], P('ep'), may hold values from -0.25 to 0.25
- expert_ids: int32 [1024, 2], P('ep'), may hold values from 0 to 7, as said below
- route_weight: float32 [1024, 2], P('ep'), may hold values from 0.2 to 1
Outputs:
- mixed: bfloat16 [1024, 2048], P('ep', 'tp')
Inputs may be any that keep to these rules, and one draw needn't show every extreme that they name: `expert_ids`: A token's two experts differ and lie in one group of 2 consecutive experts. In each aligned block of 32 rows no expert is named more than 16 times, and in every block all experts of one group, the same group for all blocks, are named exactly 16 times.
All inputs are finite; a program needn't handle non-finite values.
Results may differ from a plain program's by a relative error of at most 0.0071.
Values may be sent and summed in bfloat16 or wider, within the bound.
No kernel may reach another device: no remote copies, remote signals or barrier semaphores. Data moves between devices by JAX's collectives and lax.ppermute only.
A program may use at most 64 MiB of HBM per device.

v0:
```python
from functools import partial

import jax
import jax.numpy as jnp
from jax import lax
from jax.sharding import PartitionSpec as P


def slot_numbers(block_ids, experts):
    flat_ids = block_ids.reshape(-1)
    hit_table = (flat_ids[:, None] == jnp.arange(experts, dtype=jnp.int32)[None, :]).astype(
        jnp.int32
    )
    earlier = jnp.cumsum(hit_table, axis=0) - hit_table
    return (flat_ids, jnp.sum(earlier * hit_table, axis=1))


def placement_matrix(flat_ids, slot_index, experts, capacity):
    target = (flat_ids * capacity + slot_index).reshape(-1, 2)
    slot_rows = jnp.arange(experts * capacity, dtype=jnp.int32)[:, None]
    first_hit = (target[:, 0][None, :] == slot_rows).astype(jnp.bfloat16)
    second_hit = (target[:, 1][None, :] == slot_rows).astype(jnp.bfloat16)
    return first_hit + second_hit


def expert_apply(row_data, gate_weight, up_weight, down_weight):
    shape_in = row_data.shape
    flat_rows = row_data.reshape(-1, shape_in[-1])
    gate_part = jnp.dot(flat_rows, gate_weight[0], preferred_element_type=jnp.float32)
    up_part = jnp.dot(flat_rows, up_weight[0], preferred_element_type=jnp.float32)
    hidden = (jax.nn.silu(gate_part) * up_part).astype(jnp.bfloat16)
    produced = jnp.dot(hidden, down_weight[0], preferred_element_type=jnp.float32).astype(
        jnp.bfloat16
    )
    return produced.reshape(shape_in[:-1] + (produced.shape[-1],))


def local(tokens, norm_gain, gate_weight, up_weight, down_weight, expert_ids, route_weight):
    tp_count = lax.axis_size("tp")
    experts = lax.axis_size("ep") * gate_weight.shape[0]
    model_width = gate_weight.shape[1]
    group_rows = tokens.shape[0]
    block_rows = group_rows // tp_count
    capacity = 4 * block_rows // experts
    tp_index = lax.axis_index("tp")
    apply_experts = partial(
        expert_apply, gate_weight=gate_weight, up_weight=up_weight, down_weight=down_weight
    )
    full_rows = lax.all_to_all(tokens, "tp", split_axis=0, concat_axis=1, tiled=True)
    block_ids = lax.dynamic_slice_in_dim(expert_ids, tp_index * block_rows, block_rows, 0)
    block_weight = lax.dynamic_slice_in_dim(route_weight, tp_index * block_rows, block_rows, 0)
    widened = full_rows.astype(jnp.float32)
    mean_square = jnp.mean(widened * widened, axis=-1, keepdims=True)
    normed = (widened * lax.rsqrt(mean_square + 1e-06) * norm_gain).astype(jnp.bfloat16)
    flat_ids, slot_index = slot_numbers(block_ids, experts)
    placing = placement_matrix(flat_ids, slot_index, experts, capacity)
    outgoing = jnp.dot(placing, normed, preferred_element_type=jnp.float32).astype(jnp.bfloat16)
    outgoing = outgoing.reshape(experts, capacity, model_width)
    produced = apply_experts(
        lax.all_to_all(outgoing, "ep", split_axis=0, concat_axis=0, tiled=True)
    )
    returned = lax.all_to_all(produced, "ep", split_axis=0, concat_axis=0, tiled=True)
    picked = jnp.take(returned.reshape(-1, model_width), flat_ids * capacity + slot_index, axis=0)
    weighted = picked.astype(jnp.float32) * block_weight.reshape(-1)[:, None]
    mixed_rows = weighted.reshape(block_rows, 2, model_width).sum(axis=1).astype(jnp.bfloat16)
    return lax.all_to_all(mixed_rows, "tp", split_axis=1, concat_axis=0, tiled=True)


def solution(mesh):
    in_specs = (
        P("ep", "tp"),
        P(),
        P("ep", None, None),
        P("ep", None, None),
        P("ep", None, None),
        P("ep", None),
        P("ep", None),
    )
    out_specs = P("ep", "tp")
    return jax.shard_map(local, mesh=mesh, in_specs=in_specs, out_specs=out_specs, check_vma=False)
```

profile of v0, /device:TPU:0, one launch (start us, length us, event | category | flops | bytes accessed | tf_op | source)
XLA Modules:
  0.0 64.8 jit_solution(1656385604178816365)
XLA Ops:
  0.0 0.0 copy-start
  0.0 5.3 %all-to-all-start = ((bf16[4,32,512]{2,1,0:T(8,128)(2,1)}), bf16[4,32,512]{2,1,0:T(8,128)(2,1)S(1)}, u32[]{:S(2)}, u32[]{:S(2)}) async-start(bf16[4,32,512]{2,1,0:T(8,128)(2,1)} %bitcast.51), calls=%async_computation | async-start | bytes 262144 | tf_op jit(solution)/shard_map/all_to_all | solution.py:49
  5.3 0.8 %broadcast_multiply_fusion = (s32[32,2]{0,1:T(2,128)S(1)}, s32[32,2]{0,1:T(2,128)S(1)}) fusion(s32[128,2]{0,1:T(2,128)} %param.12, s32[]{:T(128)S(6)} %select_n.26), kind=kLoop, calls=%fused_computation.44 | loop fusion | flops 64 | bytes 772 | tf_op jit(solution)/shard_map/mul | solution.py:63
  6.1 0.1 copy.21
  6.2 0.1 reshape.87
  6.3 0.1 fusion.29
  6.3 0.1 reduce_window_sum.11
  6.4 0.2 select_reduce_fusion
  6.6 0.1 reduce_sum.32
  6.7 0.1 copy.22
  6.9 3.5 %all-to-all-done = bf16[4,32,512]{2,1,0:T(8,128)(2,1)S(1)} async-done(((bf16[4,32,512]{2,1,0:T(8,128)(2,1)}), bf16[4,32,512]{2,1,0:T(8,128)(2,1)S(1)}, u32[]{:S(2)}, u32[]{:S(2)}) %all-to-all-start) | async-done | bytes 131104 | tf_op jit(solution)/shard_map/all_to_all | solution.py:49
  10.3 0.0 copy-start.1
  10.4 0.1 fusion.13
  10.6 1.2 %convolution_convert_fusion.1 = bf16[128,2048]{1,0:T(8,128)(2,1)S(1)} fusion(f32[32,2048]{1,0:T(8,128)S(1)} %bitcast.47, f32[2048]{0:T(1024)} %param.8, f32[32]{0:T(128)S(1)} %add_rsqrt_fusion, s32[32]{0:T(128)S(1)} %get-tuple-element.10, s32[32]{0:T(128)S(1)} %get-tuple-element.9), kind=kOutput, calls=%fused_computation.2 | convolution fusion | flops 17268736 | bytes 795008 | tf_op jit(solution)/shard_map/dot_general | solution.py:57
  11.7 20.0 %all_to_all.39 = bf16[8,16,2048]{2,1,0:T(8,128)(2,1)S(1)} all-to-all(bf16[8,16,2048]{2,1,0:T(8,128)(2,1)S(1)} %bitcast.46), channel_id=1, replica_groups=mesh['ep'=8,'tp'=4] {'ep'}, dimensions={0} | all-to-all | bytes 1048576 | tf_op jit(solution)/shard_map/all_to_all | solution.py:60
  31.7 0.0 copy-done.1
  31.7 0.4 fusion.3
  32.2 0.0 copy-done
  32.2 0.0 copy-start.2
  32.2 3.2 %convolution_convert_fusion = bf16[128,2048]{1,0:T(8,128)(2,1)} fusion(bf16[1,512,2048]{2,1,0:T(8,128)(2,1)S(1)} %copy-done, bf16[128,2048]{1,0:T(8,128)(2,1)S(1)} %bitcast.45, bf16[1,2048,512]{2,1,0:T(8,128)(2,1)} %param.10, f32[128,512]{1,0:T(8,128)S(1)} %fusion.3), kind=kOutput, calls=%fused_computation.1 | convolution fusion | flops 537526272 | bytes 5505024 | tf_op jit(solution)/shard_map/dot_general | solution.py:32
  35.4 3.5 %all-to-all-start.2 = ((bf16[8,16,2048]{2,1,0:T(8,128)(2,1)}), bf16[8,16,2048]{2,1,0:T(8,128)(2,1)S(1)}, u32[]{:S(2)}, u32[]{:S(2)}) async-start(bf16[8,16,2048]{2,1,0:T(8,128)(2,1)} %bitcast.9), calls=%async_computation.2 | async-start | bytes 1048576 | tf_op jit(solution)/shard_map/all_to_all | solution.py:62
  38.9 0.1 copy.25
  39.0 0.1 mul.72
  39.1 0.1 copy.23
  39.2 0.0 copy-done.2
  39.2 0.1 constant_dynamic-slice_fusion
  39.3 0.1 copy.26
  39.4 14.8 %all-to-all-done.2 = bf16[8,16,2048]{2,1,0:T(8,128)(2,1)S(1)} async-done(((bf16[8,16,2048]{2,1,0:T(8,128)(2,1)}), bf16[8,16,2048]{2,1,0:T(8,128)(2,1)S(1)}, u32[]{:S(2)}, u32[]{:S(2)}) %all-to-all-start.2) | async-done | bytes 524320 | tf_op jit(solution)/shard_map/all_to_all | solution.py:62
  54.2 0.7 %gather_fusion = bf16[64,2048]{1,0:T(8,128)(2,1)S(1)} fusion(bf16[128,2048]{1,0:T(8,128)(2,1)S(1)} %bitcast.43, s32[1024]{0:T(1024)S(1)} %pad_clamp_fusion), kind=kCustom, calls=%fused_computation | custom fusion | bytes 524544 | tf_op jit(solution)/shard_map/jit(_take)/gather | solution.py:63
  54.9 0.2 gather.7
  55.1 1.6 %multiply_reduce_fusion = bf16[32,2048]{1,0:T(8,128)(2,1)S(1)} fusion(bf16[32,2,2048]{2,1,0:T(2,128)(2,1)S(1)} %gather.7, pred[32,2]{1,0:T(8,128)(4,1)S(1)} %copy.23, f32[32,2]{1,0:T(8,128)S(1)} %copy.26), kind=kLoop, calls=%fused_computation.10 | loop fusion | flops 458752 | bytes 393536 | tf_op jit(solution)/shard_map/reduce_sum | solution.py:65
  56.8 7.4 %all_to_all.40 = bf16[32,4,512]{2,0,1:T(8,128)(2,1)S(1)} all-to-all(bf16[32,4,512]{2,0,1:T(8,128)(2,1)S(1)} %bitcast.49), channel_id=1, replica_groups=mesh['ep'=8,'tp'=4] {'tp'}, dimensions={1} | all-to-all | bytes 262144 | tf_op jit(solution)/shard_map/all_to_all | solution.py:66
  64.2 0.7 %copy.33 = bf16[128,512]{1,0:T(8,128)(2,1)} copy(bf16[128,512]{1,0:T(8,128)(2,1)S(1)} %bitcast.50) | data formatting | bytes 262144
  (8 shorter events, 0.1 us)
Async XLA Ops:
  0.0 32.2 %copy-start = (bf16[1,512,2048]{2,1,0:T(8,128)(2,1)S(1)}, bf16[1,512,2048]{2,1,0:T(8,128)(2,1)}, u32[]{:S(2)}) copy-start(bf16[1,512,2048]{2,1,0:T(8,128)(2,1)} %param.11) | copy-start | bytes 6291460
  0.0 10.3 %all-to-all-start = ((bf16[4,32,512]{2,1,0:T(8,128)(2,1)}), bf16[4,32,512]{2,1,0:T(8,128)(2,1)S(1)}, u32[]{:S(2)}, u32[]{:S(2)}) async-start(bf16[4,32,512]{2,1,0:T(8,128)(2,1)} %bitcast.51), calls=%async_computation | async-start | bytes 262144 | tf_op jit(solution)/shard_map/all_to_all | solution.py:49
  10.3 21.4 %copy-start.1 = (bf16[1,2048,512]{2,1,0:T(8,128)(2,1)S(1)}, bf16[1,2048,512]{2,1,0:T(8,128)(2,1)}, u32[]{:S(2)}) copy-start(bf16[1,2048,512]{2,1,0:T(8,128)(2,1)} %param.9) | copy-start | bytes 6291460
  32.2 7.0 %copy-start.2 = (f32[128,2]{0,1:T(2,128)S(1)}, f32[128,2]{0,1:T(2,128)}, u32[]{:S(2)}) copy-start(f32[128,2]{0,1:T(2,128)} %param.13) | copy-start | bytes 3076
  35.4 18.8 %all-to-all-start.2 = ((bf16[8,16,2048]{2,1,0:T(8,128)(2,1)}), bf16[8,16,2048]{2,1,0:T(8,128)(2,1)S(1)}, u32[]{:S(2)}, u32[]{:S(2)}) async-start(bf16[8,16,2048]{2,1,0:T(8,128)(2,1)} %bitcast.9), calls=%async_computation.2 | async-start | bytes 1048576 | tf_op jit(solution)/shard_map/all_to_all | solution.py:62
where the time goes:
time: 65.3 us; the launch traced here: 64.8 us
  blocking collectives  27.4 us (42%)
  waiting for transfers between devices  18.3 us (28%)
  starting transfers between devices  8.81 us (13%)
  matrix products  4.82 us (7%)
  other arithmetic  2.93 us (4%)
  local copies, waits for them, and re-layouts  2.47 us (4%)
    all_to_all x1, blocking collectives, local(): lax.all_to_all(outgoing, 'ep', split_axis=0, concat_axis=0, tiled=True)  20 us
    all_to_all x1, waiting for transfers between devices, local(): lax.all_to_all(produced, 'ep', split_axis=0, concat_axis=0, tiled=True)  14.8 us
    all_to_all x1, blocking collectives, local(): lax.all_to_all(mixed_rows, 'tp', split_axis=1, concat_axis=0, tiled=True)  7.41 us
    all_to_all x1, starting transfers between devices, local(): lax.all_to_all(tokens, 'tp', split_axis=0, concat_axis=1, tiled=True)  5.32 us
    all_to_all x1, waiting for transfers between devices, local(): lax.all_to_all(tokens, 'tp', split_axis=0, concat_axis=1, tiled=True)  3.49 us
    all_to_all x1, starting transfers between devices, local(): lax.all_to_all(produced, 'ep', split_axis=0, concat_axis=0, tiled=True)  3.49 us
    dot_general x1, matrix products, expert_apply(): jnp.dot(hidden, down_weight[0], preferred_element_type=jnp.float32)  3.22 us
    reduce_sum x1, other arithmetic, local(): weighted.reshape(block_rows, 2, model_width).sum(axis=1)  1.63 us
  transfers between devices with their start and end apart: 2, of which 2 were waited for; matrix products, arithmetic and copies ran while one was open for 3% of the time, Pallas kernels for 0%

commit v1 on v0

v1 whole, which is shorter than its diff:
```python
from functools import partial

import jax
import jax.numpy as jnp
from jax import lax
from jax.experimental import pallas as pl
from jax.experimental.pallas import tpu as pltpu
from jax.sharding import PartitionSpec as P


F32 = jnp.float32
BF16 = jnp.bfloat16
LANES = 128
VMEM = pl.BlockSpec(memory_space=pltpu.VMEM)


def slot_numbers(block_ids, experts):
    flat_ids = block_ids.reshape(-1)
    hit_table = (flat_ids[:, None] == jnp.arange(experts, dtype=jnp.int32)[None, :]).astype(
        jnp.int32
    )
    earlier = jnp.cumsum(hit_table, axis=0) - hit_table
    return (flat_ids, jnp.sum(earlier * hit_table, axis=1))


def placement_matrix(flat_ids, slot_index, experts, capacity):
    target = (flat_ids * capacity + slot_index).reshape(-1, 2)
    slot_rows = jnp.arange(experts * capacity, dtype=jnp.int32)[:, None]
    first_hit = (target[:, 0][None, :] == slot_rows).astype(BF16)
    second_hit = (target[:, 1][None, :] == slot_rows).astype(BF16)
    return first_hit + second_hit


def expert_apply(row_data, gate_weight, up_weight, down_weight):
    shape_in = row_data.shape
    flat_rows = row_data.reshape(-1, shape_in[-1])
    gate_part = jnp.dot(flat_rows, gate_weight[0], preferred_element_type=F32)
    up_part = jnp.dot(flat_rows, up_weight[0], preferred_element_type=F32)
    hidden = (jax.nn.silu(gate_part) * up_part).astype(BF16)
    produced = jnp.dot(hidden, down_weight[0], preferred_element_type=F32).astype(BF16)
    return produced.reshape(shape_in[:-1] + (produced.shape[-1],))


def local_any(tokens, norm_gain, gate_weight, up_weight, down_weight, expert_ids, route_weight):
    tp_count = lax.axis_size("tp")
    experts = lax.axis_size("ep") * gate_weight.shape[0]
    model_width = gate_weight.shape[1]
    group_rows = tokens.shape[0]
    block_rows = group_rows // tp_count
    capacity = 4 * block_rows // experts
    tp_index = lax.axis_index("tp")
    apply_experts = partial(
        expert_apply, gate_weight=gate_weight, up_weight=up_weight, down_weight=down_weight
    )
    full_rows = lax.all_to_all(tokens, "tp", split_axis=0, concat_axis=1, tiled=True)
    block_ids = lax.dynamic_slice_in_dim(expert_ids, tp_index * block_rows, block_rows, 0)
    block_weight = lax.dynamic_slice_in_dim(route_weight, tp_index * block_rows, block_rows, 0)
    widened = full_rows.astype(F32)
    mean_square = jnp.mean(widened * widened, axis=-1, keepdims=True)
    normed = (widened * lax.rsqrt(mean_square + 1e-06) * norm_gain).astype(BF16)
    flat_ids, slot_index = slot_numbers(block_ids, experts)
    placing = placement_matrix(flat_ids, slot_index, experts, capacity)
    outgoing = jnp.dot(placing, normed, preferred_element_type=F32).astype(BF16)
    outgoing = outgoing.reshape(experts, capacity, model_width)
    produced = apply_experts(
        lax.all_to_all(outgoing, "ep", split_axis=0, concat_axis=0, tiled=True)
    )
    returned = lax.all_to_all(produced, "ep", split_axis=0, concat_axis=0, tiled=True)
    picked = jnp.take(returned.reshape(-1, model_width), flat_ids * capacity + slot_index, axis=0)
    weighted = picked.astype(F32) * block_weight.reshape(-1)[:, None]
    mixed_rows = weighted.reshape(block_rows, 2, model_width).sum(axis=1).astype(BF16)
    return lax.all_to_all(mixed_rows, "tp", split_axis=1, concat_axis=0, tiled=True)


def routing_kernel(
    groups, capacity, ids_ref, weight_ref, gain_in_ref, place_ref, code_ref, gain_ref
):
    gain_ref[...] = gain_in_ref[...]
    me = lax.axis_index("ep")
    chip, core = me // 2, me % 2
    rows = ids_ref.shape[1]
    slots = groups * capacity
    first = ids_ref[0:1, :]
    relative = (first >> 1) ^ chip
    hot = (relative == lax.broadcasted_iota(jnp.int32, (groups, rows), 0)).astype(F32)
    before = (
        lax.broadcasted_iota(jnp.int32, (rows, rows), 0)
        < lax.broadcasted_iota(jnp.int32, (rows, rows), 1)
    ).astype(F32)
    rank = jnp.dot(hot, before, preferred_element_type=F32)
    position = lax.broadcasted_iota(jnp.int32, (capacity, rows), 0).astype(F32)
    place = jnp.concatenate(
        [
            jnp.where(rank[k : k + 1] == position, 1.0, 0.0) * hot[k : k + 1]
            for k in range(groups)
        ],
        axis=0,
    )
    place_ref[...] = place.astype(BF16)
    mine = (first & 1) == core
    lane = lax.broadcasted_iota(jnp.int32, (slots, LANES), 1)
    code = jnp.zeros((slots, LANES), F32)
    for which, row in enumerate(
        (
            jnp.where(mine, weight_ref[0:1, :], weight_ref[1:2, :]),
            jnp.where(mine, weight_ref[1:2, :], weight_ref[0:1, :]),
        )
    ):
        rest = jnp.sum(place * row, axis=1, keepdims=True)
        for part in range(3):
            piece = rest.astype(BF16).astype(F32)
            rest = rest - piece
            code = jnp.where(lane == 3 * which + part, piece, code)
    code_ref[...] = code.astype(BF16)


def dispatch_kernel(count, groups, capacity, *refs):
    parts, (gain_ref, place_ref, code_ref), outs = refs[:count], refs[count : count + 3], refs[count + 3 :]
    me = lax.axis_index("tp")
    width = parts[0].shape[1]
    wide = [p[...].astype(F32) for p in parts]
    square = sum(jnp.sum(w * w, axis=1, keepdims=True) for w in wide)
    scale = lax.rsqrt(square / (width * count) + 1e-06)
    place = place_ref[...]
    for k in range(count):
        at = pl.ds(pl.multiple_of((me ^ k) * width, width), width)
        normed = (wide[k] * scale * gain_ref[:, at]).astype(BF16)
        placed = jnp.dot(place, normed, preferred_element_type=F32).astype(BF16)
        for g in range(groups):
            outs[g][:, at] = placed[g * capacity : (g + 1) * capacity]
    for g in range(groups):
        outs[g][:, width * count :] = code_ref[g * capacity : (g + 1) * capacity, :]


def expert_kernel(groups, width, *refs):
    rows, weights, outs = refs[:groups], refs[groups : groups + 6], refs[groups + 6 :]
    x = jnp.concatenate([r[:, :width] for r in rows], axis=0)
    code = jnp.concatenate([r[:, width:] for r in rows], axis=0).astype(F32)
    total = None
    for which in range(2):
        gate_ref, up_ref, down_ref = weights[3 * which : 3 * which + 3]
        gate = jnp.dot(x, gate_ref[0], preferred_element_type=F32)
        up = jnp.dot(x, up_ref[0], preferred_element_type=F32)
        hidden = (gate / (1.0 + jnp.exp(-gate)) * up).astype(BF16)
        made = jnp.dot(hidden, down_ref[0], preferred_element_type=F32).astype(BF16)
        at = 3 * which
        weight = code[:, at : at + 1] + code[:, at + 1 : at + 2] + code[:, at + 2 : at + 3]
        term = made.astype(F32) * weight
        total = term if total is None else total + term
    mixed = total.astype(BF16)
    capacity = rows[0].shape[0]
    for g in range(groups):
        outs[g][...] = mixed[g * capacity : (g + 1) * capacity]


def restore_kernel(count, groups, *refs):
    rows, place_ref, outs = refs[:groups], refs[groups], refs[groups + 1 :]
    me = lax.axis_index("tp")
    width = outs[0].shape[1]
    back = place_ref[...].astype(F32).T.astype(BF16)
    for k in range(count):
        at = pl.ds(pl.multiple_of((me ^ k) * width, width), width)
        got = jnp.concatenate([r[:, at] for r in rows], axis=0)
        outs[k][...] = jnp.dot(back, got, preferred_element_type=F32).astype(BF16)


def assemble_kernel(count, *refs):
    parts, out_ref = refs[:count], refs[count]
    me = lax.axis_index("tp")
    rows = parts[0].shape[0]
    for k in range(count):
        out_ref[pl.ds(pl.multiple_of((me ^ k) * rows, rows), rows), :] = parts[k][...]


def call(kernel, outs, args, flops, limit=4 << 20):
    return pl.pallas_call(
        kernel,
        out_shape=outs,
        in_specs=[VMEM] * len(args),
        out_specs=jax.tree.map(lambda _: VMEM, outs),
        compiler_params=pltpu.CompilerParams(vmem_limit_bytes=limit),
        cost_estimate=pl.CostEstimate(flops=flops, bytes_accessed=1 << 20, transcendentals=0),
    )(*args)


def exchange(array, axis, size, mask):
    return lax.ppermute(array, axis, [(i, i ^ mask) for i in range(size)])


def exchange_all(pieces, axis, size, stride):
    got = {0: pieces[0]}
    for k in range(1, len(pieces)):
        got[k] = exchange(pieces[k], axis, size, stride * k)
    return [got[k] for k in range(len(pieces))]


def local_pairs(tokens, norm_gain, gate_weight, up_weight, down_weight, expert_ids, route_weight):
    tp_count = lax.axis_size("tp")
    ep_count = lax.axis_size("ep")
    groups = ep_count // 2
    width = gate_weight.shape[1]
    part = tokens.shape[1]
    block = tokens.shape[0] // tp_count
    capacity = 4 * block // ep_count
    slots = groups * capacity
    tp_index = lax.axis_index("tp")
    weights = (gate_weight, up_weight, down_weight)

    mine = [
        lax.dynamic_slice_in_dim(tokens, (tp_index ^ k) * block, block, 0) for k in range(tp_count)
    ]
    parts = exchange_all(mine, "tp", tp_count, 1)
    others = []
    for w in weights:
        others.append(exchange(w, "ep", ep_count, 1))

    ids = lax.dynamic_slice_in_dim(expert_ids.T, tp_index * block, block, 1)
    route = lax.dynamic_slice_in_dim(route_weight.T, tp_index * block, block, 1)
    place, code, gain = call(
        partial(routing_kernel, groups, capacity),
        (
            jax.ShapeDtypeStruct((slots, block), BF16),
            jax.ShapeDtypeStruct((slots, LANES), BF16),
            jax.ShapeDtypeStruct((1, width), F32),
        ),
        (ids, route, norm_gain.reshape(1, -1)),
        1 << 33,
    )
    row = jax.ShapeDtypeStruct((capacity, width + LANES), BF16)
    sent = call(
        partial(dispatch_kernel, tp_count, groups, capacity),
        (row,) * groups,
        (*parts, gain, place, code),
        1 << 24,
    )
    arrived = exchange_all(sent, "ep", ep_count, 2)
    made = call(
        partial(expert_kernel, groups, width),
        (jax.ShapeDtypeStruct((capacity, width), BF16),) * groups,
        (*arrived, *weights, *others),
        1 << 30,
        8 << 20,
    )
    returned = exchange_all(made, "ep", ep_count, 2)
    slices = call(
        partial(restore_kernel, tp_count, groups),
        (jax.ShapeDtypeStruct((block, part), BF16),) * tp_count,
        (*returned, place),
        1 << 24,
    )
    final = exchange_all(slices, "tp", tp_count, 1)
    return call(
        partial(assemble_kernel, tp_count),
        jax.ShapeDtypeStruct(tokens.shape, BF16),
        final,
        1 << 20,
    )


def solution(mesh):
    in_specs = (
        P("ep", "tp"),
        P(),
        P("ep", None, None),
        P("ep", None, None),
        P("ep", None, None),
        P("ep", None),
        P("ep", None),
    )
    group_experts = mesh.shape["tp"] // 2
    pairs = group_experts == 2

    def body(*arrays):
        return (local_pairs if pairs else local_any)(*arrays)

    return jax.shard_map(
        body, mesh=mesh, in_specs=in_specs, out_specs=P("ep", "tp"), check_vma=False
    )
```

time: 65.3 us -> 46.7 us (0.72)
  blocking collectives: 27.4 us -> 0 us
  starting transfers between devices: 8.81 us -> 23.2 us
  Pallas kernels: 0 us -> 6.12 us
  matrix products: 4.82 us -> 0 us
  waiting for transfers between devices: 18.3 us -> 14.8 us
  other arithmetic: 2.93 us -> 0 us
    all_to_all x2 -> x0, blocking collectives: 27.4 us -> none  [the longest x1 20 us: local(): lax.all_to_all(outgoing, 'ep', split_axis=0, concat_axis=0, tiled=True)]
    ppermute x0 -> x15, starting transfers between devices: none -> 23.2 us  [exchange(): return lax.ppermute(array, axis, [(i, i ^ mask) for i in range(size)])]
    all_to_all x2 -> x0, waiting for transfers between devices: 18.3 us -> none  [the longest x1 14.8 us: local(): lax.all_to_all(produced, 'ep', split_axis=0, concat_axis=0, tiled=True)]
    ppermute x0 -> x15, waiting for transfers between devices: none -> 14.8 us  [exchange(): return lax.ppermute(array, axis, [(i, i ^ mask) for i in range(size)])]
    all_to_all x2 -> x0, starting transfers between devices: 8.81 us -> none  [the longest x1 5.32 us: local(): lax.all_to_all(tokens, 'tp', split_axis=0, concat_axis=1, tiled=True)]
    pallas_call x0 -> x5, Pallas kernels: none -> 6.12 us  [call(): pl.pallas_call(kernel, out_shape=outs, in_specs=[VMEM] * len(args), out_s...]
    dot_general x3 -> x0, matrix products: 4.82 us -> none  [the longest x1 3.22 us: expert_apply(): jnp.dot(hidden, down_weight[0], preferred_element_type=jnp.float32)]
    reduce_sum x3 -> x0, other arithmetic: 1.95 us -> none  [the longest x1 1.63 us: local(): weighted.reshape(block_rows, 2, model_width).sum(axis=1)]
  transfers between devices with their start and end apart: 2 -> 15, of which waited for: 2 -> 10; matrix products, arithmetic and copies ran while one was open for 3% -> 4% of each run, Pallas kernels for 0% -> 1%
where the time goes in v1:
time: 46.7 us; the launch traced here: 46.5 us
  starting transfers between devices  23.2 us (50%)
  waiting for transfers between devices  14.8 us (32%)
  Pallas kernels  6.12 us (13%)
  local copies, waits for them, and re-layouts  2.35 us (5%)
    ppermute x15, starting transfers between devices, exchange(): return lax.ppermute(array, axis, [(i, i ^ mask) for i in range(size)])  23.2 us
    ppermute x15, waiting for transfers between devices, exchange(): return lax.ppermute(array, axis, [(i, i ^ mask) for i in range(size)])  14.8 us
    pallas_call x5, Pallas kernels, call(): pl.pallas_call(kernel, out_shape=outs, in_specs=[VMEM] * len(args), out_s...  6.12 us
  transfers between devices with their start and end apart: 15, of which 10 were waited for; matrix products, arithmetic and copies ran while one was open for 4% of the time, Pallas kernels for 1%

profile of v1, /device:TPU:0, one launch (start us, length us, event | category | flops | bytes accessed | tf_op | source)
XLA Modules:
  0.0 46.5 jit_solution(18371081915242858313)
XLA Ops:
  0.0 0.0 copy-start
  0.0 0.5 %collective-permute-start.6 = (bf16[1,2048,512]{2,1,0:T(8,128)(2,1)}, bf16[1,2048,512]{2,1,0:T(8,128)(2,1)S(1)}, u32[]{:S(2)}, u32[]{:S(2)}) collective-permute-start(bf16[1,2048,512]{2,1,0:T(8,128)(2,1)} %refs_4_.1), channel_id=1, source_target_pairs={{0,4},{4,0},{8,12},{12,8},{16,20},{20,16},{24,28},{28,24},{1,5},{5... | collective-permute-start | bytes 6291464 | tf_op jit(solution)/shard_map/ppermute | solution.py:187
  0.5 0.1 collective-permute-start.7
  0.6 0.4 collective-permute-start.8
  1.0 0.8 %constant_dynamic-slice_fusion.2 = (bf16[32,512]{1,0:T(8,128)(2,1)S(1)}, bf16[32,512]{1,0:T(8,128)(2,1)S(1)}, bf16[32,512]{1,0:T(8,128)(2,1)S(1)}, bf16[32,512]{1,0:T(8,128)(2,1)S(1)}) fusion(bf16[128,512]{1,0:T(8,128)(2,1)} %param.7, s32[]{:T(128)S(6)} %select_n.17, s32[]{:T(128)S(6)} %select_n.15, s32[]{:T(128)S(6)} %select_n.14, s32[]{:T(128)S(6)} %select_n.16), kind=kLoop, calls=%fused_computation.2 | loop fusion | bytes 262160 | tf_op jit(solution)/shard_map/dynamic_slice | solution.py:210
  1.8 3.6 %collective-permute-start.2 = (bf16[32,512]{1,0:T(8,128)(2,1)S(1)}, bf16[32,512]{1,0:T(8,128)(2,1)S(1)}, u32[]{:S(2)}, u32[]{:S(2)}) collective-permute-start(bf16[32,512]{1,0:T(8,128)(2,1)S(1)} %get-tuple-element.35), channel_id=1, source_target_pairs={{0,3},{1,2},{2,1},{3,0},{4,7},{5,6},{6,5},{7,4},{8,11},{9,10},{10,... | collective-permute-start | bytes 98312 | tf_op jit(solution)/shard_map/ppermute | solution.py:187
  5.4 0.5 %collective-permute-start = (bf16[32,512]{1,0:T(8,128)(2,1)S(1)}, bf16[32,512]{1,0:T(8,128)(2,1)S(1)}, u32[]{:S(2)}, u32[]{:S(2)}) collective-permute-start(bf16[32,512]{1,0:T(8,128)(2,1)S(1)} %get-tuple-element.36), channel_id=1, source_target_pairs={{0,1},{1,0},{2,3},{3,2},{4,5},{5,4},{6,7},{7,6},{8,9},{9,8},{10,11... | collective-permute-start | bytes 98312 | tf_op jit(solution)/shard_map/ppermute | solution.py:187
  5.9 0.0 copy-done
  5.9 0.1 fusion.ids_ref
  6.0 0.8 %fusion.1.weight_ref = f32[2,32]{1,0:T(2,128)S(1)} fusion(f32[128,2]{0,1:T(2,128)} %param.13, s32[]{:T(128)S(6)} %select_n.14), kind=kLoop, calls=%fused_computation.7 | loop fusion | bytes 516 | tf_op jit(solution)/shard_map/dynamic_slice | solution.py:218
  6.8 0.6 %collective-permute-done.2.refs_3_ = bf16[32,512]{1,0:T(8,128)(2,1)S(1)} collective-permute-done((bf16[32,512]{1,0:T(8,128)(2,1)S(1)}, bf16[32,512]{1,0:T(8,128)(2,1)S(1)}, u32[]{:S(2)}, u32[]{:S(2)}) %collective-permute-start.2) | collective-permute-done | bytes 32800 | tf_op jit(solution)/shard_map/ppermute | solution.py:187
  7.4 1.9 %collective-permute-start.1 = (bf16[32,512]{1,0:T(8,128)(2,1)S(1)}, bf16[32,512]{1,0:T(8,128)(2,1)S(1)}, u32[]{:S(2)}, u32[]{:S(2)}) collective-permute-start(bf16[32,512]{1,0:T(8,128)(2,1)S(1)} %get-tuple-element.38), channel_id=1, source_target_pairs={{0,2},{1,3},{2,0},{3,1},{4,6},{5,7},{6,4},{7,5},{8,10},{9,11},{10,... | collective-permute-start | bytes 98312 | tf_op jit(solution)/shard_map/ppermute | solution.py:187
  9.3 0.0 copy-start.4
  9.3 0.7 %copy-done.4 = f32[2048]{0:T(1024)S(1)} copy-done((f32[2048]{0:T(1024)S(1)}, f32[2048]{0:T(1024)}, u32[]{:S(2)}) %copy-start.4) | copy-done | bytes 8216
  10.0 0.0 copy-start.1
  10.0 0.0 copy-start.2
  10.0 0.0 copy-start.3
  10.0 0.2 shard_map.73
  10.2 0.0 collective-permute-done.refs_1_
  10.2 1.1 %collective-permute-done.1.refs_2_ = bf16[32,512]{1,0:T(8,128)(2,1)S(1)} collective-permute-done((bf16[32,512]{1,0:T(8,128)(2,1)S(1)}, bf16[32,512]{1,0:T(8,128)(2,1)S(1)}, u32[]{:S(2)}, u32[]{:S(2)}) %collective-permute-start.1) | collective-permute-done | bytes 32800 | tf_op jit(solution)/shard_map/ppermute | solution.py:187
  11.3 0.3 shard_map.74
  11.6 2.0 %collective-permute-start.3 = (bf16[16,2176]{1,0:T(8,128)(2,1)S(1)}, bf16[16,2176]{1,0:T(8,128)(2,1)S(1)}, u32[]{:S(2)}, u32[]{:S(2)}) collective-permute-start(bf16[16,2176]{1,0:T(8,128)(2,1)S(1)} %get-tuple-element.24), channel_id=1, source_target_pairs={{0,8},{4,12},{8,0},{12,4},{16,24},{20,28},{24,16},{28,20},{1,9},{5... | collective-permute-start | bytes 208904 | tf_op jit(solution)/shard_map/ppermute | solution.py:187
  13.6 2.6 %collective-permute-start.4 = (bf16[16,2176]{1,0:T(8,128)(2,1)S(1)}, bf16[16,2176]{1,0:T(8,128)(2,1)S(1)}, u32[]{:S(2)}, u32[]{:S(2)}) collective-permute-start(bf16[16,2176]{1,0:T(8,128)(2,1)S(1)} %get-tuple-element.25), channel_id=1, source_target_pairs={{0,16},{4,20},{8,24},{12,28},{16,0},{20,4},{24,8},{28,12},{1,17},{... | collective-permute-start | bytes 208904 | tf_op jit(solution)/shard_map/ppermute | solution.py:187
  16.2 0.2 collective-permute-done.3.refs_1_
  16.4 3.6 %collective-permute-start.5 = (bf16[16,2176]{1,0:T(8,128)(2,1)S(1)}, bf16[16,2176]{1,0:T(8,128)(2,1)S(1)}, u32[]{:S(2)}, u32[]{:S(2)}) collective-permute-start(bf16[16,2176]{1,0:T(8,128)(2,1)S(1)} %get-tuple-element.26), channel_id=1, source_target_pairs={{0,24},{4,28},{8,16},{12,20},{16,8},{20,12},{24,0},{28,4},{1,25},{... | collective-permute-start | bytes 208904 | tf_op jit(solution)/shard_map/ppermute | solution.py:187
  20.0 0.4 collective-permute-done.4.refs_2_
  20.3 2.3 %collective-permute-done.5.refs_3_ = bf16[16,2176]{1,0:T(8,128)(2,1)S(1)} collective-permute-done((bf16[16,2176]{1,0:T(8,128)(2,1)S(1)}, bf16[16,2176]{1,0:T(8,128)(2,1)S(1)}, u32[]{:S(2)}, u32[]{:S(2)}) %collective-permute-start.5) | collective-permute-done | bytes 69664 | tf_op jit(solution)/shard_map/ppermute | solution.py:187
  22.6 0.0 collective-permute-done.6.refs_7_
  22.6 0.0 collective-permute-done.7.refs_8_
  22.6 0.0 collective-permute-done.8.refs_9_
  22.6 0.0 copy-done.1
  22.6 0.0 copy-done.2
  22.7 0.0 copy-done.3
  22.7 4.7 %shard_map.75 = (bf16[16,2048]{1,0:T(8,128)(2,1)S(1)}, bf16[16,2048]{1,0:T(8,128)(2,1)S(1)}, bf16[16,2048]{1,0:T(8,128)(2,1)S(1)}, bf16[16,2048]{1,0:T(8,128)(2,1)S(1)}) custom-call(bf16[16,2176]{1,0:T(8,128)(2,1)S(1)} %get-tuple-element.23.refs_0_, bf16[16,2176]{1,0:T(8,128)(2,1)S(1)} %collective-permute-done.3.refs_1_, ...), custom_call_target="tpu_custom_call" | custom-call | flops 1073741824 | bytes 1048576 | tf_op jit(solution)/shard_map/pallas_call | solution.py:176
  27.4 0.7 %collective-permute-start.9 = (bf16[16,2048]{1,0:T(8,128)(2,1)S(1)}, bf16[16,2048]{1,0:T(8,128)(2,1)S(1)}, u32[]{:S(2)}, u32[]{:S(2)}) collective-permute-start(bf16[16,2048]{1,0:T(8,128)(2,1)S(1)} %get-tuple-element.28), channel_id=1, source_target_pairs={{0,8},{4,12},{8,0},{12,4},{16,24},{20,28},{24,16},{28,20},{1,9},{5... | collective-permute-start | bytes 196616 | tf_op jit(solution)/shard_map/ppermute | solution.py:187
  28.0 3.4 %collective-permute-start.10 = (bf16[16,2048]{1,0:T(8,128)(2,1)S(1)}, bf16[16,2048]{1,0:T(8,128)(2,1)S(1)}, u32[]{:S(2)}, u32[]{:S(2)}) collective-permute-start(bf16[16,2048]{1,0:T(8,128)(2,1)S(1)} %get-tuple-element.29), channel_id=1, source_target_pairs={{0,16},{4,20},{8,24},{12,28},{16,0},{20,4},{24,8},{28,12},{1,17},{... | collective-permute-start | bytes 196616 | tf_op jit(solution)/shard_map/ppermute | solution.py:187
  31.4 0.4 collective-permute-start.11
  31.8 0.0 collective-permute-done.9.refs_1_
  31.8 2.6 %collective-permute-done.10.refs_2_ = bf16[16,2048]{1,0:T(8,128)(2,1)S(1)} collective-permute-done((bf16[16,2048]{1,0:T(8,128)(2,1)S(1)}, bf16[16,2048]{1,0:T(8,128)(2,1)S(1)}, u32[]{:S(2)}, u32[]{:S(2)}) %collective-permute-start.10) | collective-permute-done | bytes 65568 | tf_op jit(solution)/shard_map/ppermute | solution.py:187
  34.4 3.1 %collective-permute-done.11.refs_3_ = bf16[16,2048]{1,0:T(8,128)(2,1)S(1)} collective-permute-done((bf16[16,2048]{1,0:T(8,128)(2,1)S(1)}, bf16[16,2048]{1,0:T(8,128)(2,1)S(1)}, u32[]{:S(2)}, u32[]{:S(2)}) %collective-permute-start.11) | collective-permute-done | bytes 65568 | tf_op jit(solution)/shard_map/ppermute | solution.py:187
  37.5 0.2 shard_map.76
  37.7 1.7 %collective-permute-start.12 = (bf16[32,512]{1,0:T(8,128)(2,1)S(1)}, bf16[32,512]{1,0:T(8,128)(2,1)S(1)}, u32[]{:S(2)}, u32[]{:S(2)}) collective-permute-start(bf16[32,512]{1,0:T(8,128)(2,1)S(1)} %get-tuple-element.32), channel_id=1, source_target_pairs={{0,1},{1,0},{2,3},{3,2},{4,5},{5,4},{6,7},{7,6},{8,9},{9,8},{10,11... | collective-permute-start | bytes 98312 | tf_op jit(solution)/shard_map/ppermute | solution.py:187
  39.5 1.5 %collective-permute-start.13 = (bf16[32,512]{1,0:T(8,128)(2,1)S(1)}, bf16[32,512]{1,0:T(8,128)(2,1)S(1)}, u32[]{:S(2)}, u32[]{:S(2)}) collective-permute-start(bf16[32,512]{1,0:T(8,128)(2,1)S(1)} %get-tuple-element.33), channel_id=1, source_target_pairs={{0,2},{1,3},{2,0},{3,1},{4,6},{5,7},{6,4},{7,5},{8,10},{9,11},{10,... | collective-permute-start | bytes 98312 | tf_op jit(solution)/shard_map/ppermute | solution.py:187
  41.0 0.3 collective-permute-start.14
  41.3 0.4 collective-permute-done.12.refs_1_
  41.7 1.7 %collective-permute-done.13.refs_2_ = bf16[32,512]{1,0:T(8,128)(2,1)S(1)} collective-permute-done((bf16[32,512]{1,0:T(8,128)(2,1)S(1)}, bf16[32,512]{1,0:T(8,128)(2,1)S(1)}, u32[]{:S(2)}, u32[]{:S(2)}) %collective-permute-start.13) | collective-permute-done | bytes 32800 | tf_op jit(solution)/shard_map/ppermute | solution.py:187
  43.4 2.4 %collective-permute-done.14.refs_3_ = bf16[32,512]{1,0:T(8,128)(2,1)S(1)} collective-permute-done((bf16[32,512]{1,0:T(8,128)(2,1)S(1)}, bf16[32,512]{1,0:T(8,128)(2,1)S(1)}, u32[]{:S(2)}, u32[]{:S(2)}) %collective-permute-start.14) | collective-permute-done | bytes 32800 | tf_op jit(solution)/shard_map/ppermute | solution.py:187
  45.8 0.7 %shard_map.77 = bf16[128,512]{1,0:T(8,128)(2,1)} custom-call(bf16[32,512]{1,0:T(8,128)(2,1)S(1)} %get-tuple-element.31.refs_0_, bf16[32,512]{1,0:T(8,128)(2,1)S(1)} %collective-permute-done.12.refs_1_, bf16[32,512]{1,0:T(8,128)(2,1)S(1)} %collective-permute-done.13.refs_2_, bf16[32,512]{1,0:T(8,128)(2,1)S(1)} %collective-permute-done.14.refs_3_), custom_call_target="tpu_custom_call" | custom-call | flops 1048576 | bytes 1048576 | tf_op jit(solution)/shard_map/pallas_call | solution.py:176
Async XLA Ops:
  0.0 5.9 %copy-start = (s32[128,2]{0,1:T(2,128)S(1)}, s32[128,2]{0,1:T(2,128)}, u32[]{:S(2)}) copy-start(s32[128,2]{0,1:T(2,128)} %param.12) | copy-start | bytes 3076
  0.0 22.6 %collective-permute-start.6 = (bf16[1,2048,512]{2,1,0:T(8,128)(2,1)}, bf16[1,2048,512]{2,1,0:T(8,128)(2,1)S(1)}, u32[]{:S(2)}, u32[]{:S(2)}) collective-permute-start(bf16[1,2048,512]{2,1,0:T(8,128)(2,1)} %refs_4_.1), channel_id=1, source_target_pairs={{0,4},{4,0},{8,12},{12,8},{16,20},{20,16},{24,28},{28,24},{1,5},{5... | collective-permute-start | bytes 6291464 | tf_op jit(solution)/shard_map/ppermute | solution.py:187
  0.5 22.1 %collective-permute-start.7 = (bf16[1,2048,512]{2,1,0:T(8,128)(2,1)}, bf16[1,2048,512]{2,1,0:T(8,128)(2,1)}, u32[]{:S(2)}, u32[]{:S(2)}) collective-permute-start(bf16[1,2048,512]{2,1,0:T(8,128)(2,1)} %refs_5_.1), channel_id=1, source_target_pairs={{0,4},{4,0},{8,12},{12,8},{16,20},{20,16},{24,28},{28,24},{1,5},{5... | collective-permute-start | bytes 6291464 | tf_op jit(solution)/shard_map/ppermute | solution.py:187
  0.6 22.1 %collective-permute-start.8 = (bf16[1,512,2048]{2,1,0:T(8,128)(2,1)}, bf16[1,512,2048]{2,1,0:T(8,128)(2,1)}, u32[]{:S(2)}, u32[]{:S(2)}) collective-permute-start(bf16[1,512,2048]{2,1,0:T(8,128)(2,1)} %refs_6_.1), channel_id=1, source_target_pairs={{0,4},{4,0},{8,12},{12,8},{16,20},{20,16},{24,28},{28,24},{1,5},{5... | collective-permute-start | bytes 6291464 | tf_op jit(solution)/shard_map/ppermute | solution.py:187
  1.8 5.6 %collective-permute-start.2 = (bf16[32,512]{1,0:T(8,128)(2,1)S(1)}, bf16[32,512]{1,0:T(8,128)(2,1)S(1)}, u32[]{:S(2)}, u32[]{:S(2)}) collective-permute-start(bf16[32,512]{1,0:T(8,128)(2,1)S(1)} %get-tuple-element.35), channel_id=1, source_target_pairs={{0,3},{1,2},{2,1},{3,0},{4,7},{5,6},{6,5},{7,4},{8,11},{9,10},{10,... | collective-permute-start | bytes 98312 | tf_op jit(solution)/shard_map/ppermute | solution.py:187
  5.4 4.8 %collective-permute-start = (bf16[32,512]{1,0:T(8,128)(2,1)S(1)}, bf16[32,512]{1,0:T(8,128)(2,1)S(1)}, u32[]{:S(2)}, u32[]{:S(2)}) collective-permute-start(bf16[32,512]{1,0:T(8,128)(2,1)S(1)} %get-tuple-element.36), channel_id=1, source_target_pairs={{0,1},{1,0},{2,3},{3,2},{4,5},{5,4},{6,7},{7,6},{8,9},{9,8},{10,11... | collective-permute-start | bytes 98312 | tf_op jit(solution)/shard_map/ppermute | solution.py:187
  7.4 3.9 %collective-permute-start.1 = (bf16[32,512]{1,0:T(8,128)(2,1)S(1)}, bf16[32,512]{1,0:T(8,128)(2,1)S(1)}, u32[]{:S(2)}, u32[]{:S(2)}) collective-permute-start(bf16[32,512]{1,0:T(8,128)(2,1)S(1)} %get-tuple-element.38), channel_id=1, source_target_pairs={{0,2},{1,3},{2,0},{3,1},{4,6},{5,7},{6,4},{7,5},{8,10},{9,11},{10,... | collective-permute-start | bytes 98312 | tf_op jit(solution)/shard_map/ppermute | solution.py:187
  9.3 0.7 %copy-start.4 = (f32[2048]{0:T(1024)S(1)}, f32[2048]{0:T(1024)}, u32[]{:S(2)}) copy-start(f32[2048]{0:T(1024)} %param.8) | copy-start | bytes 24580
  10.0 12.7 %copy-start.1 = (bf16[1,2048,512]{2,1,0:T(8,128)(2,1)S(1)}, bf16[1,2048,512]{2,1,0:T(8,128)(2,1)}, u32[]{:S(2)}) copy-start(bf16[1,2048,512]{2,1,0:T(8,128)(2,1)} %refs_4_.1) | copy-start | bytes 6291460
  10.0 12.7 %copy-start.2 = (bf16[1,2048,512]{2,1,0:T(8,128)(2,1)S(1)}, bf16[1,2048,512]{2,1,0:T(8,128)(2,1)}, u32[]{:S(2)}) copy-start(bf16[1,2048,512]{2,1,0:T(8,128)(2,1)} %refs_5_.1) | copy-start | bytes 6291460
  10.0 12.7 %copy-start.3 = (bf16[1,512,2048]{2,1,0:T(8,128)(2,1)S(1)}, bf16[1,512,2048]{2,1,0:T(8,128)(2,1)}, u32[]{:S(2)}) copy-start(bf16[1,512,2048]{2,1,0:T(8,128)(2,1)} %refs_6_.1) | copy-start | bytes 6291460
  11.6 4.8 %collective-permute-start.3 = (bf16[16,2176]{1,0:T(8,128)(2,1)S(1)}, bf16[16,2176]{1,0:T(8,128)(2,1)S(1)}, u32[]{:S(2)}, u32[]{:S(2)}) collective-permute-start(bf16[16,2176]{1,0:T(8,128)(2,1)S(1)} %get-tuple-element.24), channel_id=1, source_target_pairs={{0,8},{4,12},{8,0},{12,4},{16,24},{20,28},{24,16},{28,20},{1,9},{5... | collective-permute-start | bytes 208904 | tf_op jit(solution)/shard_map/ppermute | solution.py:187
  13.6 6.7 %collective-permute-start.4 = (bf16[16,2176]{1,0:T(8,128)(2,1)S(1)}, bf16[16,2176]{1,0:T(8,128)(2,1)S(1)}, u32[]{:S(2)}, u32[]{:S(2)}) collective-permute-start(bf16[16,2176]{1,0:T(8,128)(2,1)S(1)} %get-tuple-element.25), channel_id=1, source_target_pairs={{0,16},{4,20},{8,24},{12,28},{16,0},{20,4},{24,8},{28,12},{1,17},{... | collective-permute-start | bytes 208904 | tf_op jit(solution)/shard_map/ppermute | solution.py:187
  16.4 6.2 %collective-permute-start.5 = (bf16[16,2176]{1,0:T(8,128)(2,1)S(1)}, bf16[16,2176]{1,0:T(8,128)(2,1)S(1)}, u32[]{:S(2)}, u32[]{:S(2)}) collective-permute-start(bf16[16,2176]{1,0:T(8,128)(2,1)S(1)} %get-tuple-element.26), channel_id=1, source_target_pairs={{0,24},{4,28},{8,16},{12,20},{16,8},{20,12},{24,0},{28,4},{1,25},{... | collective-permute-start | bytes 208904 | tf_op jit(solution)/shard_map/ppermute | solution.py:187
  27.4 4.5 %collective-permute-start.9 = (bf16[16,2048]{1,0:T(8,128)(2,1)S(1)}, bf16[16,2048]{1,0:T(8,128)(2,1)S(1)}, u32[]{:S(2)}, u32[]{:S(2)}) collective-permute-start(bf16[16,2048]{1,0:T(8,128)(2,1)S(1)} %get-tuple-element.28), channel_id=1, source_target_pairs={{0,8},{4,12},{8,0},{12,4},{16,24},{20,28},{24,16},{28,20},{1,9},{5... | collective-permute-start | bytes 196616 | tf_op jit(solution)/shard_map/ppermute | solution.py:187
  28.0 6.4 %collective-permute-start.10 = (bf16[16,2048]{1,0:T(8,128)(2,1)S(1)}, bf16[16,2048]{1,0:T(8,128)(2,1)S(1)}, u32[]{:S(2)}, u32[]{:S(2)}) collective-permute-start(bf16[16,2048]{1,0:T(8,128)(2,1)S(1)} %get-tuple-element.29), channel_id=1, source_target_pairs={{0,16},{4,20},{8,24},{12,28},{16,0},{20,4},{24,8},{28,12},{1,17},{... | collective-permute-start | bytes 196616 | tf_op jit(solution)/shard_map/ppermute | solution.py:187
  31.4 6.1 %collective-permute-start.11 = (bf16[16,2048]{1,0:T(8,128)(2,1)S(1)}, bf16[16,2048]{1,0:T(8,128)(2,1)S(1)}, u32[]{:S(2)}, u32[]{:S(2)}) collective-permute-start(bf16[16,2048]{1,0:T(8,128)(2,1)S(1)} %get-tuple-element.30), channel_id=1, source_target_pairs={{0,24},{4,28},{8,16},{12,20},{16,8},{20,12},{24,0},{28,4},{1,25},{... | collective-permute-start | bytes 196616 | tf_op jit(solution)/shard_map/ppermute | solution.py:187
  37.7 4.0 %collective-permute-start.12 = (bf16[32,512]{1,0:T(8,128)(2,1)S(1)}, bf16[32,512]{1,0:T(8,128)(2,1)S(1)}, u32[]{:S(2)}, u32[]{:S(2)}) collective-permute-start(bf16[32,512]{1,0:T(8,128)(2,1)S(1)} %get-tuple-element.32), channel_id=1, source_target_pairs={{0,1},{1,0},{2,3},{3,2},{4,5},{5,4},{6,7},{7,6},{8,9},{9,8},{10,11... | collective-permute-start | bytes 98312 | tf_op jit(solution)/shard_map/ppermute | solution.py:187
  39.5 3.9 %collective-permute-start.13 = (bf16[32,512]{1,0:T(8,128)(2,1)S(1)}, bf16[32,512]{1,0:T(8,128)(2,1)S(1)}, u32[]{:S(2)}, u32[]{:S(2)}) collective-permute-start(bf16[32,512]{1,0:T(8,128)(2,1)S(1)} %get-tuple-element.33), channel_id=1, source_target_pairs={{0,2},{1,3},{2,0},{3,1},{4,6},{5,7},{6,4},{7,5},{8,10},{9,11},{10,... | collective-permute-start | bytes 98312 | tf_op jit(solution)/shard_map/ppermute | solution.py:187
  41.0 4.8 %collective-permute-start.14 = (bf16[32,512]{1,0:T(8,128)(2,1)S(1)}, bf16[32,512]{1,0:T(8,128)(2,1)S(1)}, u32[]{:S(2)}, u32[]{:S(2)}) collective-permute-start(bf16[32,512]{1,0:T(8,128)(2,1)S(1)} %get-tuple-element.34), channel_id=1, source_target_pairs={{0,3},{1,2},{2,1},{3,0},{4,7},{5,6},{6,5},{7,4},{8,11},{9,10},{10,... | collective-permute-start | bytes 98312 | tf_op jit(solution)/shard_map/ppermute | solution.py:187

commit v2 on v1

--- a/solution.py
+++ b/solution.py
@@ -73,51 +73,64 @@
 
 
 def routing_kernel(
-    groups, capacity, ids_ref, weight_ref, gain_in_ref, place_ref, code_ref, gain_ref
+    groups, capacity, block, ids_ref, place_ref, wide_ref, back_ref, first_ref
 ):
-    gain_ref[...] = gain_in_ref[...]
-    me = lax.axis_index("ep")
-    chip, core = me // 2, me % 2
+    chip = lax.axis_index("ep") // 2
+    column = lax.axis_index("tp")
     rows = ids_ref.shape[1]
-    slots = groups * capacity
+    columns = rows // block
     first = ids_ref[0:1, :]
-    relative = (first >> 1) ^ chip
-    hot = (relative == lax.broadcasted_iota(jnp.int32, (groups, rows), 0)).astype(F32)
-    before = (
-        lax.broadcasted_iota(jnp.int32, (rows, rows), 0)
-        < lax.broadcasted_iota(jnp.int32, (rows, rows), 1)
-    ).astype(F32)
-    rank = jnp.dot(hot, before, preferred_element_type=F32)
+    first_ref[...] = first
+    group = first >> 1
+    bin_of = group * columns + lax.broadcasted_iota(jnp.int32, (1, rows), 1) // block
+    bins = groups * columns
+    hot = bin_of == lax.broadcasted_iota(jnp.int32, (bins, rows), 0)
+    before = lax.broadcasted_iota(jnp.int32, (rows, rows), 0) < lax.broadcasted_iota(
+        jnp.int32, (rows, rows), 1
+    )
+    ahead = jnp.dot(
+        hot.astype(F32).astype(BF16), before.astype(F32).astype(BF16), preferred_element_type=F32
+    )
+    rank = jnp.sum(jnp.where(hot, ahead, 0.0), axis=0, keepdims=True)
     position = lax.broadcasted_iota(jnp.int32, (capacity, rows), 0).astype(F32)
-    place = jnp.concatenate(
-        [
-            jnp.where(rank[k : k + 1] == position, 1.0, 0.0) * hot[k : k + 1]
-            for k in range(groups)
-        ],
-        axis=0,
-    )
-    place_ref[...] = place.astype(BF16)
+    at = rank == position
+
+    def placed(which):
+        return jnp.where(at & (bin_of == which), 1.0, 0.0)
+
+    full = jnp.concatenate([placed(n) for n in range(bins)], axis=0)
+    back_ref[...] = full.T.astype(BF16)
+    wide = jnp.concatenate(
+        [placed((k ^ chip) * columns + column) for k in range(groups)], axis=0
+    )
+    wide_ref[...] = wide.astype(BF16)
+    place_ref[...] = pltpu.roll(wide, rows - column * block, 1)[:, :block].astype(BF16)
+
+
+def code_of(wide, first, route, core):
     mine = (first & 1) == core
-    lane = lax.broadcasted_iota(jnp.int32, (slots, LANES), 1)
-    code = jnp.zeros((slots, LANES), F32)
-    for which, row in enumerate(
-        (
-            jnp.where(mine, weight_ref[0:1, :], weight_ref[1:2, :]),
-            jnp.where(mine, weight_ref[1:2, :], weight_ref[0:1, :]),
-        )
-    ):
-        rest = jnp.sum(place * row, axis=1, keepdims=True)
+    lane = lax.broadcasted_iota(jnp.int32, (wide.shape[0], LANES), 1)
+    code = jnp.zeros(lane.shape, F32)
+    for which in range(2):
+        row = jnp.where(mine, route[which : which + 1], route[1 - which : 2 - which])
+        rest = jnp.sum(wide * row, axis=1, keepdims=True)
         for part in range(3):
             piece = rest.astype(BF16).astype(F32)
             rest = rest - piece
             code = jnp.where(lane == 3 * which + part, piece, code)
-    code_ref[...] = code.astype(BF16)
+    return code.astype(BF16)
 
 
 def dispatch_kernel(count, groups, capacity, *refs):
-    parts, (gain_ref, place_ref, code_ref), outs = refs[:count], refs[count : count + 3], refs[count + 3 :]
+    parts, (gain_ref, place_ref, wide_ref, first_ref, route_ref), outs = (
+        refs[:count],
+        refs[count : count + 5],
+        refs[count + 5 :],
+    )
     me = lax.axis_index("tp")
+    core = lax.axis_index("ep") % 2
     width = parts[0].shape[1]
+    code = code_of(wide_ref[...].astype(F32), first_ref[...], route_ref[...], core)
     wide = [p[...].astype(F32) for p in parts]
     square = sum(jnp.sum(w * w, axis=1, keepdims=True) for w in wide)
     scale = lax.rsqrt(square / (width * count) + 1e-06)
@@ -129,11 +142,11 @@
         for g in range(groups):
             outs[g][:, at] = placed[g * capacity : (g + 1) * capacity]
     for g in range(groups):
-        outs[g][:, width * count :] = code_ref[g * capacity : (g + 1) * capacity, :]
+        outs[g][:, width * count :] = code[g * capacity : (g + 1) * capacity]
 
 
 def expert_kernel(groups, width, *refs):
-    rows, weights, outs = refs[:groups], refs[groups : groups + 6], refs[groups + 6 :]
+    rows, weights, out_ref = refs[:groups], refs[groups : groups + 6], refs[groups + 6]
     x = jnp.concatenate([r[:, :width] for r in rows], axis=0)
     code = jnp.concatenate([r[:, width:] for r in rows], axis=0).astype(F32)
     total = None
@@ -148,28 +161,19 @@
         term = made.astype(F32) * weight
         total = term if total is None else total + term
     mixed = total.astype(BF16)
-    capacity = rows[0].shape[0]
+    chip = lax.axis_index("ep") // 2
+    capacity, part = out_ref.shape[1:]
+    columns = width // part
     for g in range(groups):
-        outs[g][...] = mixed[g * capacity : (g + 1) * capacity]
-
-
-def restore_kernel(count, groups, *refs):
-    rows, place_ref, outs = refs[:groups], refs[groups], refs[groups + 1 :]
-    me = lax.axis_index("tp")
-    width = outs[0].shape[1]
-    back = place_ref[...].astype(F32).T.astype(BF16)
-    for k in range(count):
-        at = pl.ds(pl.multiple_of((me ^ k) * width, width), width)
-        got = jnp.concatenate([r[:, at] for r in rows], axis=0)
-        outs[k][...] = jnp.dot(back, got, preferred_element_type=F32).astype(BF16)
-
-
-def assemble_kernel(count, *refs):
-    parts, out_ref = refs[:count], refs[count]
-    me = lax.axis_index("tp")
-    rows = parts[0].shape[0]
-    for k in range(count):
-        out_ref[pl.ds(pl.multiple_of((me ^ k) * rows, rows), rows), :] = parts[k][...]
+        for n in range(columns):
+            out_ref[(g ^ chip) * columns + n] = mixed[
+                g * capacity : (g + 1) * capacity, n * part : (n + 1) * part
+            ]
+
+
+def restore_kernel(rows_ref, back_ref, out_ref):
+    rows = rows_ref[...].reshape(-1, rows_ref.shape[-1])
+    out_ref[...] = jnp.dot(back_ref[...], rows, preferred_element_type=F32).astype(BF16)
 
 
 def call(kernel, outs, args, flops, limit=4 << 20):
@@ -200,7 +204,8 @@
     groups = ep_count // 2
     width = gate_weight.shape[1]
     part = tokens.shape[1]
-    block = tokens.shape[0] // tp_count
+    all_rows = tokens.shape[0]
+    block = all_rows // tp_count
     capacity = 4 * block // ep_count
     slots = groups * capacity
     tp_index = lax.axis_index("tp")
@@ -214,46 +219,43 @@
     for w in weights:
         others.append(exchange(w, "ep", ep_count, 1))
 
-    ids = lax.dynamic_slice_in_dim(expert_ids.T, tp_index * block, block, 1)
-    route = lax.dynamic_slice_in_dim(route_weight.T, tp_index * block, block, 1)
-    place, code, gain = call(
-        partial(routing_kernel, groups, capacity),
+    ids, route = expert_ids.T, route_weight.T
+    bins = groups * tp_count
+    place, wide, back, first = call(
+        partial(routing_kernel, groups, capacity, block),
         (
             jax.ShapeDtypeStruct((slots, block), BF16),
-            jax.ShapeDtypeStruct((slots, LANES), BF16),
-            jax.ShapeDtypeStruct((1, width), F32),
+            jax.ShapeDtypeStruct((slots, all_rows), BF16),
+            jax.ShapeDtypeStruct((all_rows, bins * capacity), BF16),
+            jax.ShapeDtypeStruct((1, all_rows), jnp.int32),
         ),
-        (ids, route, norm_gain.reshape(1, -1)),
+        (ids,),
         1 << 33,
     )
     row = jax.ShapeDtypeStruct((capacity, width + LANES), BF16)
     sent = call(
         partial(dispatch_kernel, tp_count, groups, capacity),
         (row,) * groups,
-        (*parts, gain, place, code),
+        (*parts, norm_gain.reshape(1, -1), place, wide, first, route),
         1 << 24,
     )
     arrived = exchange_all(sent, "ep", ep_count, 2)
     made = call(
         partial(expert_kernel, groups, width),
-        (jax.ShapeDtypeStruct((capacity, width), BF16),) * groups,
+        jax.ShapeDtypeStruct((bins, capacity, part), BF16),
         (*arrived, *weights, *others),
         1 << 30,
         8 << 20,
     )
-    returned = exchange_all(made, "ep", ep_count, 2)
-    slices = call(
-        partial(restore_kernel, tp_count, groups),
-        (jax.ShapeDtypeStruct((block, part), BF16),) * tp_count,
-        (*returned, place),
-        1 << 24,
-    )
-    final = exchange_all(slices, "tp", tp_count, 1)
+    homes = [
+        [(chip * 2 + core) * tp_count + column for chip in range(groups) for column in range(tp_count)]
+        for core in range(2)
+    ]
+    returned = lax.all_to_all(
+        made, ("ep", "tp"), split_axis=0, concat_axis=0, tiled=True, axis_index_groups=homes
+    )
     return call(
-        partial(assemble_kernel, tp_count),
-        jax.ShapeDtypeStruct(tokens.shape, BF16),
-        final,
-        1 << 20,
+        restore_kernel, jax.ShapeDtypeStruct(tokens.shape, BF16), (returned, back), 1 << 25
     )
 
 

time: 46.7 us -> 43.6 us (0.934)
  blocking collectives: 0 us -> 15.2 us
  waiting for transfers between devices: 14.8 us -> 5.63 us
  starting transfers between devices: 23.2 us -> 14.9 us
  local copies, waits for them, and re-layouts: 2.35 us -> 1.52 us
    all_to_all x0 -> x1, blocking collectives: none -> 15.2 us  [local_pairs(): lax.all_to_all(made, ('ep', 'tp'), split_axis=0, concat_axis=0, tiled=Tru...]
    ppermute x15 -> x9, waiting for transfers between devices: 14.8 us -> 5.63 us  [exchange(): return lax.ppermute(array, axis, [(i, i ^ mask) for i in range(size)])]
    ppermute x15 -> x9, starting transfers between devices: 23.2 us -> 14.9 us  [exchange(): return lax.ppermute(array, axis, [(i, i ^ mask) for i in range(size)])]
    dynamic_slice x2 -> x0, local copies, waits for them, and re-layouts: 0.82 us -> none  [the longest x1 0.75 us: local_pairs(): route = lax.dynamic_slice_in_dim(route_weight.T, tp_index * block, block, 1)]
    pallas_call x5 -> x4, Pallas kernels: 6.12 us -> 6.09 us  [call(): pl.pallas_call(kernel, out_shape=outs, in_specs=[VMEM] * len(args), out_s...]
  transfers between devices with their start and end apart: 15 -> 9, of which waited for: 10 -> 5; matrix products, arithmetic and copies ran while one was open for 4% -> 2% of each run, Pallas kernels for 1% -> 1%
where the time goes in v2:
time: 43.6 us; the launch traced here: 43.4 us
  blocking collectives  15.2 us (35%)
  starting transfers between devices  14.9 us (34%)
  Pallas kernels  6.09 us (14%)
  waiting for transfers between devices  5.63 us (13%)
  local copies, waits for them, and re-layouts  1.52 us (3%)
    all_to_all x1, blocking collectives, local_pairs(): lax.all_to_all(made, ('ep', 'tp'), split_axis=0, concat_axis=0, tiled=Tru...  15.2 us
    ppermute x9, starting transfers between devices, exchange(): return lax.ppermute(array, axis, [(i, i ^ mask) for i in range(size)])  14.9 us
    pallas_call x4, Pallas kernels, call(): pl.pallas_call(kernel, out_shape=outs, in_specs=[VMEM] * len(args), out_s...  6.09 us
    ppermute x9, waiting for transfers between devices, exchange(): return lax.ppermute(array, axis, [(i, i ^ mask) for i in range(size)])  5.63 us
  transfers between devices with their start and end apart: 9, of which 5 were waited for; matrix products, arithmetic and copies ran while one was open for 2% of the time, Pallas kernels for 1%

profile of v2, /device:TPU:0, one launch (start us, length us, event | category | flops | bytes accessed | tf_op | source)
XLA Modules:
  0.0 43.4 jit_solution(11018259947779523373)
XLA Ops:
  0.0 0.5 %collective-permute-start.6 = (bf16[1,2048,512]{2,1,0:T(8,128)(2,1)}, bf16[1,2048,512]{2,1,0:T(8,128)(2,1)S(1)}, u32[]{:S(2)}, u32[]{:S(2)}) collective-permute-start(bf16[1,2048,512]{2,1,0:T(8,128)(2,1)} %refs_4_.1), channel_id=1, source_target_pairs={{0,4},{4,0},{8,12},{12,8},{16,20},{20,16},{24,28},{28,24},{1,5},{5... | collective-permute-start | bytes 6291464 | tf_op jit(solution)/shard_map/ppermute | solution.py:191
  0.5 0.0 collective-permute-start.7
  0.5 0.5 %collective-permute-start.8 = (bf16[1,512,2048]{2,1,0:T(8,128)(2,1)}, bf16[1,512,2048]{2,1,0:T(8,128)(2,1)}, u32[]{:S(2)}, u32[]{:S(2)}) collective-permute-start(bf16[1,512,2048]{2,1,0:T(8,128)(2,1)} %refs_6_.1), channel_id=1, source_target_pairs={{0,4},{4,0},{8,12},{12,8},{16,20},{20,16},{24,28},{28,24},{1,5},{5... | collective-permute-start | bytes 6291464 | tf_op jit(solution)/shard_map/ppermute | solution.py:191
  1.0 0.8 %constant_dynamic-slice_fusion = (bf16[32,512]{1,0:T(8,128)(2,1)S(1)}, bf16[32,512]{1,0:T(8,128)(2,1)S(1)}, bf16[32,512]{1,0:T(8,128)(2,1)S(1)}, bf16[32,512]{1,0:T(8,128)(2,1)S(1)}) fusion(bf16[128,512]{1,0:T(8,128)(2,1)} %param.7, s32[]{:T(128)S(6)} %select_n.15, s32[]{:T(128)S(6)} %select_n.13, s32[]{:T(128)S(6)} %select_n.12, s32[]{:T(128)S(6)} %select_n.14), kind=kLoop, calls=%fused_computation | loop fusion | bytes 262160 | tf_op jit(solution)/shard_map/dynamic_slice | solution.py:215
  1.8 3.5 %collective-permute-start.2 = (bf16[32,512]{1,0:T(8,128)(2,1)S(1)}, bf16[32,512]{1,0:T(8,128)(2,1)S(1)}, u32[]{:S(2)}, u32[]{:S(2)}) collective-permute-start(bf16[32,512]{1,0:T(8,128)(2,1)S(1)} %get-tuple-element.21), channel_id=1, source_target_pairs={{0,3},{1,2},{2,1},{3,0},{4,7},{5,6},{6,5},{7,4},{8,11},{9,10},{10,... | collective-permute-start | bytes 98312 | tf_op jit(solution)/shard_map/ppermute | solution.py:191
  5.3 0.5 %collective-permute-start = (bf16[32,512]{1,0:T(8,128)(2,1)S(1)}, bf16[32,512]{1,0:T(8,128)(2,1)S(1)}, u32[]{:S(2)}, u32[]{:S(2)}) collective-permute-start(bf16[32,512]{1,0:T(8,128)(2,1)S(1)} %get-tuple-element.22), channel_id=1, source_target_pairs={{0,1},{1,0},{2,3},{3,2},{4,5},{5,4},{6,7},{7,6},{8,9},{9,8},{10,11... | collective-permute-start | bytes 98312 | tf_op jit(solution)/shard_map/ppermute | solution.py:191
  5.9 1.5 %collective-permute-done.2.refs_3_ = bf16[32,512]{1,0:T(8,128)(2,1)S(1)} collective-permute-done((bf16[32,512]{1,0:T(8,128)(2,1)S(1)}, bf16[32,512]{1,0:T(8,128)(2,1)S(1)}, u32[]{:S(2)}, u32[]{:S(2)}) %collective-permute-start.2) | collective-permute-done | bytes 32800 | tf_op jit(solution)/shard_map/ppermute | solution.py:191
  7.4 1.8 %collective-permute-start.1 = (bf16[32,512]{1,0:T(8,128)(2,1)S(1)}, bf16[32,512]{1,0:T(8,128)(2,1)S(1)}, u32[]{:S(2)}, u32[]{:S(2)}) collective-permute-start(bf16[32,512]{1,0:T(8,128)(2,1)S(1)} %get-tuple-element.24), channel_id=1, source_target_pairs={{0,2},{1,3},{2,0},{3,1},{4,6},{5,7},{6,4},{7,5},{8,10},{9,11},{10,... | collective-permute-start | bytes 98312 | tf_op jit(solution)/shard_map/ppermute | solution.py:191
  9.2 0.0 copy-start.5
  9.2 0.7 %copy-done.5 = s32[128,2]{0,1:T(2,128)S(1)} copy-done((s32[128,2]{0,1:T(2,128)S(1)}, s32[128,2]{0,1:T(2,128)}, u32[]{:S(2)}) %copy-start.5) | copy-done | bytes 1048
  9.9 0.0 copy-start.3
  9.9 0.0 copy-start.4
  9.9 0.0 copy-start
  9.9 0.0 copy-start.1
  9.9 0.0 copy-start.2
  9.9 0.2 shard_map.73
  10.2 0.0 collective-permute-done.refs_1_
  10.2 1.1 %collective-permute-done.1.refs_2_ = bf16[32,512]{1,0:T(8,128)(2,1)S(1)} collective-permute-done((bf16[32,512]{1,0:T(8,128)(2,1)S(1)}, bf16[32,512]{1,0:T(8,128)(2,1)S(1)}, u32[]{:S(2)}, u32[]{:S(2)}) %collective-permute-start.1) | collective-permute-done | bytes 32800 | tf_op jit(solution)/shard_map/ppermute | solution.py:191
  11.3 0.0 copy-done.3
  11.3 0.0 copy-done.4
  11.3 0.3 shard_map.74
  11.6 1.9 %collective-permute-start.3 = (bf16[16,2176]{1,0:T(8,128)(2,1)S(1)}, bf16[16,2176]{1,0:T(8,128)(2,1)S(1)}, u32[]{:S(2)}, u32[]{:S(2)}) collective-permute-start(bf16[16,2176]{1,0:T(8,128)(2,1)S(1)} %get-tuple-element.17), channel_id=1, source_target_pairs={{0,8},{4,12},{8,0},{12,4},{16,24},{20,28},{24,16},{28,20},{1,9},{5... | collective-permute-start | bytes 208904 | tf_op jit(solution)/shard_map/ppermute | solution.py:191
  13.6 2.6 %collective-permute-start.4 = (bf16[16,2176]{1,0:T(8,128)(2,1)S(1)}, bf16[16,2176]{1,0:T(8,128)(2,1)S(1)}, u32[]{:S(2)}, u32[]{:S(2)}) collective-permute-start(bf16[16,2176]{1,0:T(8,128)(2,1)S(1)} %get-tuple-element.18), channel_id=1, source_target_pairs={{0,16},{4,20},{8,24},{12,28},{16,0},{20,4},{24,8},{28,12},{1,17},{... | collective-permute-start | bytes 208904 | tf_op jit(solution)/shard_map/ppermute | solution.py:191
  16.2 0.3 collective-permute-done.3.refs_1_
  16.4 3.5 %collective-permute-start.5 = (bf16[16,2176]{1,0:T(8,128)(2,1)S(1)}, bf16[16,2176]{1,0:T(8,128)(2,1)S(1)}, u32[]{:S(2)}, u32[]{:S(2)}) collective-permute-start(bf16[16,2176]{1,0:T(8,128)(2,1)S(1)} %get-tuple-element.19), channel_id=1, source_target_pairs={{0,24},{4,28},{8,16},{12,20},{16,8},{20,12},{24,0},{28,4},{1,25},{... | collective-permute-start | bytes 208904 | tf_op jit(solution)/shard_map/ppermute | solution.py:191
  19.9 0.4 collective-permute-done.4.refs_2_
  20.3 2.3 %collective-permute-done.5.refs_3_ = bf16[16,2176]{1,0:T(8,128)(2,1)S(1)} collective-permute-done((bf16[16,2176]{1,0:T(8,128)(2,1)S(1)}, bf16[16,2176]{1,0:T(8,128)(2,1)S(1)}, u32[]{:S(2)}, u32[]{:S(2)}) %collective-permute-start.5) | collective-permute-done | bytes 69664 | tf_op jit(solution)/shard_map/ppermute | solution.py:191
  22.6 0.0 collective-permute-done.6.refs_7_
  22.6 0.0 collective-permute-done.7.refs_8_
  22.6 0.0 collective-permute-done.8.refs_9_
  22.6 0.0 copy-done
  22.6 0.0 copy-done.1
  22.7 0.0 copy-done.2
  22.7 4.7 %shard_map.75 = bf16[16,16,512]{2,1,0:T(8,128)(2,1)S(1)} custom-call(bf16[16,2176]{1,0:T(8,128)(2,1)S(1)} %get-tuple-element.16.refs_0_, bf16[16,2176]{1,0:T(8,128)(2,1)S(1)} %collective-permute-done.3.refs_1_, bf16[16,2176]{1,0:T(8,128)(2,1)S(1)} %collective-permute-done.4.refs_2_, bf16[16,2176]{1,0:T(8,128)(2,1)S(1)} %collective-permute-done.5.refs_3_, ...), custom_call_target="tpu_custom_call" | custom-call | flops 1073741824 | bytes 1048576 | tf_op jit(solution)/shard_map/pallas_call | solution.py:180
  27.4 15.2 %all_to_all.5.rows_ref = bf16[16,16,512]{2,1,0:T(8,128)(2,1)S(1)} all-to-all(bf16[16,16,512]{2,1,0:T(8,128)(2,1)S(1)} %shard_map.75), channel_id=1, replica_groups={{0,1,2,3,8,9,10,11,16,17,18,19,24,25,26,27},{4,5,6,7,12,13,14,15,20,21,..., dimensions={0} | all-to-all | bytes 524288 | tf_op jit(solution)/shard_map/all_to_all | solution.py:254
  42.6 0.8 %shard_map.76 = bf16[128,512]{1,0:T(8,128)(2,1)} custom-call(bf16[16,16,512]{2,1,0:T(8,128)(2,1)S(1)} %all_to_all.5.rows_ref, bf16[128,256]{1,0:T(8,128)(2,1)S(1)} %get-tuple-element.20.back_ref), custom_call_target="tpu_custom_call" | custom-call | flops 33554432 | bytes 1048576 | tf_op jit(solution)/shard_map/pallas_call | solution.py:180
Async XLA Ops:
  0.0 22.6 %collective-permute-start.6 = (bf16[1,2048,512]{2,1,0:T(8,128)(2,1)}, bf16[1,2048,512]{2,1,0:T(8,128)(2,1)S(1)}, u32[]{:S(2)}, u32[]{:S(2)}) collective-permute-start(bf16[1,2048,512]{2,1,0:T(8,128)(2,1)} %refs_4_.1), channel_id=1, source_target_pairs={{0,4},{4,0},{8,12},{12,8},{16,20},{20,16},{24,28},{28,24},{1,5},{5... | collective-permute-start | bytes 6291464 | tf_op jit(solution)/shard_map/ppermute | solution.py:191
  0.5 22.1 %collective-permute-start.7 = (bf16[1,2048,512]{2,1,0:T(8,128)(2,1)}, bf16[1,2048,512]{2,1,0:T(8,128)(2,1)}, u32[]{:S(2)}, u32[]{:S(2)}) collective-permute-start(bf16[1,2048,512]{2,1,0:T(8,128)(2,1)} %refs_5_.1), channel_id=1, source_target_pairs={{0,4},{4,0},{8,12},{12,8},{16,20},{20,16},{24,28},{28,24},{1,5},{5... | collective-permute-start | bytes 6291464 | tf_op jit(solution)/shard_map/ppermute | solution.py:191
  0.5 22.1 %collective-permute-start.8 = (bf16[1,512,2048]{2,1,0:T(8,128)(2,1)}, bf16[1,512,2048]{2,1,0:T(8,128)(2,1)}, u32[]{:S(2)}, u32[]{:S(2)}) collective-permute-start(bf16[1,512,2048]{2,1,0:T(8,128)(2,1)} %refs_6_.1), channel_id=1, source_target_pairs={{0,4},{4,0},{8,12},{12,8},{16,20},{20,16},{24,28},{28,24},{1,5},{5... | collective-permute-start | bytes 6291464 | tf_op jit(solution)/shard_map/ppermute | solution.py:191
  1.8 5.6 %collective-permute-start.2 = (bf16[32,512]{1,0:T(8,128)(2,1)S(1)}, bf16[32,512]{1,0:T(8,128)(2,1)S(1)}, u32[]{:S(2)}, u32[]{:S(2)}) collective-permute-start(bf16[32,512]{1,0:T(8,128)(2,1)S(1)} %get-tuple-element.21), channel_id=1, source_target_pairs={{0,3},{1,2},{2,1},{3,0},{4,7},{5,6},{6,5},{7,4},{8,11},{9,10},{10,... | collective-permute-start | bytes 98312 | tf_op jit(solution)/shard_map/ppermute | solution.py:191
  5.3 4.8 %collective-permute-start = (bf16[32,512]{1,0:T(8,128)(2,1)S(1)}, bf16[32,512]{1,0:T(8,128)(2,1)S(1)}, u32[]{:S(2)}, u32[]{:S(2)}) collective-permute-start(bf16[32,512]{1,0:T(8,128)(2,1)S(1)} %get-tuple-element.22), channel_id=1, source_target_pairs={{0,1},{1,0},{2,3},{3,2},{4,5},{5,4},{6,7},{7,6},{8,9},{9,8},{10,11... | collective-permute-start | bytes 98312 | tf_op jit(solution)/shard_map/ppermute | solution.py:191
  7.4 3.9 %collective-permute-start.1 = (bf16[32,512]{1,0:T(8,128)(2,1)S(1)}, bf16[32,512]{1,0:T(8,128)(2,1)S(1)}, u32[]{:S(2)}, u32[]{:S(2)}) collective-permute-start(bf16[32,512]{1,0:T(8,128)(2,1)S(1)} %get-tuple-element.24), channel_id=1, source_target_pairs={{0,2},{1,3},{2,0},{3,1},{4,6},{5,7},{6,4},{7,5},{8,10},{9,11},{10,... | collective-permute-start | bytes 98312 | tf_op jit(solution)/shard_map/ppermute | solution.py:191
  9.2 0.7 %copy-start.5 = (s32[128,2]{0,1:T(2,128)S(1)}, s32[128,2]{0,1:T(2,128)}, u32[]{:S(2)}) copy-start(s32[128,2]{0,1:T(2,128)} %param.12) | copy-start | bytes 3076
  9.9 1.4 %copy-start.3 = (f32[2048]{0:T(1024)S(1)}, f32[2048]{0:T(1024)}, u32[]{:S(2)}) copy-start(f32[2048]{0:T(1024)} %param.8) | copy-start | bytes 24580
  9.9 1.4 %copy-start.4 = (f32[128,2]{0,1:T(2,128)S(1)}, f32[128,2]{0,1:T(2,128)}, u32[]{:S(2)}) copy-start(f32[128,2]{0,1:T(2,128)} %param.13) | copy-start | bytes 3076
  9.9 12.7 %copy-start = (bf16[1,2048,512]{2,1,0:T(8,128)(2,1)S(1)}, bf16[1,2048,512]{2,1,0:T(8,128)(2,1)}, u32[]{:S(2)}) copy-start(bf16[1,2048,512]{2,1,0:T(8,128)(2,1)} %refs_4_.1) | copy-start | bytes 6291460
  9.9 12.8 %copy-start.1 = (bf16[1,2048,512]{2,1,0:T(8,128)(2,1)S(1)}, bf16[1,2048,512]{2,1,0:T(8,128)(2,1)}, u32[]{:S(2)}) copy-start(bf16[1,2048,512]{2,1,0:T(8,128)(2,1)} %refs_5_.1) | copy-start | bytes 6291460
  9.9 12.8 %copy-start.2 = (bf16[1,512,2048]{2,1,0:T(8,128)(2,1)S(1)}, bf16[1,512,2048]{2,1,0:T(8,128)(2,1)}, u32[]{:S(2)}) copy-start(bf16[1,512,2048]{2,1,0:T(8,128)(2,1)} %refs_6_.1) | copy-start | bytes 6291460
  11.6 4.8 %collective-permute-start.3 = (bf16[16,2176]{1,0:T(8,128)(2,1)S(1)}, bf16[16,2176]{1,0:T(8,128)(2,1)S(1)}, u32[]{:S(2)}, u32[]{:S(2)}) collective-permute-start(bf16[16,2176]{1,0:T(8,128)(2,1)S(1)} %get-tuple-element.17), channel_id=1, source_target_pairs={{0,8},{4,12},{8,0},{12,4},{16,24},{20,28},{24,16},{28,20},{1,9},{5... | collective-permute-start | bytes 208904 | tf_op jit(solution)/shard_map/ppermute | solution.py:191
  13.6 6.7 %collective-permute-start.4 = (bf16[16,2176]{1,0:T(8,128)(2,1)S(1)}, bf16[16,2176]{1,0:T(8,128)(2,1)S(1)}, u32[]{:S(2)}, u32[]{:S(2)}) collective-permute-start(bf16[16,2176]{1,0:T(8,128)(2,1)S(1)} %get-tuple-element.18), channel_id=1, source_target_pairs={{0,16},{4,20},{8,24},{12,28},{16,0},{20,4},{24,8},{28,12},{1,17},{... | collective-permute-start | bytes 208904 | tf_op jit(solution)/shard_map/ppermute | solution.py:191
  16.4 6.2 %collective-permute-start.5 = (bf16[16,2176]{1,0:T(8,128)(2,1)S(1)}, bf16[16,2176]{1,0:T(8,128)(2,1)S(1)}, u32[]{:S(2)}, u32[]{:S(2)}) collective-permute-start(bf16[16,2176]{1,0:T(8,128)(2,1)S(1)} %get-tuple-element.19), channel_id=1, source_target_pairs={{0,24},{4,28},{8,16},{12,20},{16,8},{20,12},{24,0},{28,4},{1,25},{... | collective-permute-start | bytes 208904 | tf_op jit(solution)/shard_map/ppermute | solution.py:191
